TPU v7x, 512 devices: a 8x2x16 block of a 8x16x16 slice. The times are simulated.
512 devices in a mesh: grp: 2 (over y), kv: 16 (over z), tp: 16 (over x, core).
Axes of the slice: x: 8, y: 2, z: 16, core: 2. Of those that a mesh axis runs over, the one named last changes fastest.
The devices are a block of a 8x16x16 slice.
Arguments:
- stream_in: bfloat16 [384, 4096], P(('grp', 'tp'), 'kv'), parts along dimension 0, may hold values from -40 to 40
- positions: int32 [384], P(('grp', 'kv')), parts along dimension 0, may hold values from 1024 to 32767
- ret_state: float32 [384, 16, 128, 128], P(('grp', 'kv'), 'tp'), parts along dimension 0, may hold values from -0.6 to 0.6
- first_gain: float32 [4096], P('kv'), may hold values from 0.1 to 1.9
- first_gate: bfloat16 [4096, 11008], P('kv', 'tp'), may hold values from -0.09375 to 0.09375
- first_up: bfloat16 [4096, 11008], P('kv', 'tp'), may hold values from -0.09375 to 0.09375
- first_down: bfloat16 [11008, 4096], P('tp', 'kv'), may hold values from -0.1875 to 0.1875
- mix_gain: float32 [4096], P('kv'), may hold values from 0.1 to 1.9
- w_query: bfloat16 [4096, 2048], P('kv', 'tp'), may hold values from -0.09375 to 0.09375
- w_key: bfloat16 [4096, 2048], P('kv', 'tp'), may hold values from -0.09375 to 0.09375
- w_value: bfloat16 [4096, 2048], P('kv', 'tp'), may hold values from -0.09375 to 0.09375
- w_outgate: bfloat16 [4096, 2048], P('kv', 'tp'), may hold values from -0.09375 to 0.09375
- w_out: bfloat16 [2048, 4096], P('tp', 'kv'), may hold values from -0.21875 to 0.21875
- head_gain: float32 [2048], P('tp'), may hold values from 0.1 to 1.9
- second_gain: float32 [4096], P('kv'), may hold values from 0.1 to 1.9
- second_gate: bfloat16 [4096, 11008], P('kv', 'tp'), may hold values from -0.09375 to 0.09375
- second_up: bfloat16 [4096, 11008], P('kv', 'tp'), may hold values from -0.09375 to 0.09375
- second_down: bfloat16 [11008, 4096], P('tp', 'kv'), may hold values from -0.1875 to 0.1875
Outputs:
- stream_out: bfloat16 [384, 4096], P(('grp', 'tp'), 'kv'), parts along dimension 0
- new_state: float32 [384, 16, 128, 128], P(('grp', 'kv'), 'tp'), parts along dimension 0
There are 2 independent parts, one for each index of `grp`. A program takes and returns all parts, laid end to end along the dimension named above; an argument that names none is the same for every part. Nothing has to cross between parts.
All inputs are finite; a program needn't handle non-finite values.
Results may differ from a plain program's by a relative error of at most 0.03.
Values may be sent and summed in bfloat16 or wider, within the bound.
No kernel may reach another device: no remote copies, remote signals or barrier semaphores. Data moves between devices by JAX's collectives and lax.ppermute only.
A program may use at most 64 MiB of HBM per device.

v0:
```python
import jax
import jax.numpy as jnp
from jax import lax
from jax.sharding import PartitionSpec as P

D = 4096
EPS_NORM = 1e-06
EPS_GROUP = 1e-05


def in_blocks(x, dim, length):
    lengths = x.shape
    parts = x.reshape(*lengths[:dim], length, lengths[dim] // length, *lengths[dim + 1 :])
    return jnp.moveaxis(parts, dim, 0)


def sent_and_summed(x, axis, dim):
    parts = in_blocks(x, dim, lax.axis_size(axis))
    arrived = lax.all_to_all(parts, axis, split_axis=0, concat_axis=0, tiled=True)
    return arrived.astype(jnp.float32).sum(axis=0)


def sent_together(arrays, axis, dim, along):
    columns = [a.reshape(*a.shape[:along], -1) for a in arrays]
    both = jnp.concatenate(columns, axis=along)
    filled, at, done = (sent_and_summed(both, axis, dim), 0, [])
    for a, column in zip(arrays, columns):
        section = filled[..., at : at + column.shape[along]]
        done.append(section.reshape(*section.shape[:along], *a.shape[along:]))
        at += column.shape[along]
    return tuple(done)


def from_everyone(x, axis):
    length = lax.axis_size(axis)
    return lax.all_to_all(jnp.broadcast_to(x[None], (length, *x.shape)), axis, 0, 0, tiled=True)


def joined_along(parts, dim):
    parts = jnp.moveaxis(parts, 0, dim)
    lengths = parts.shape
    return parts.reshape(*lengths[:dim], lengths[dim] * lengths[dim + 1], *lengths[dim + 2 :])


def collect(x, axis, dim):
    parts = from_everyone(x, axis)
    return joined_along(parts, dim)


def widen_rows(stream_rows):
    return lax.all_gather(stream_rows, "tp", axis=0, tiled=True)


def prepare(stream, norm_gain):
    widened = stream.astype(jnp.float32)
    squares = jnp.sum(widened * widened, axis=1)
    scaled = (widened * norm_gain).astype(jnp.bfloat16)
    return (squares, scaled)


def feed_forward(stream, norm_gain, w_gate, w_up):
    squares, scaled = prepare(stream, norm_gain)
    gate_part = jnp.dot(scaled, w_gate, preferred_element_type=jnp.float32)
    up_part = jnp.dot(scaled, w_up, preferred_element_type=jnp.float32)
    gate_part, up_part, squares = sent_together(
        (
            gate_part.astype(jnp.bfloat16),
            up_part.astype(jnp.bfloat16),
            squares.astype(jnp.bfloat16),
        ),
        "kv",
        0,
        1,
    )
    factor = lax.rsqrt(squares / D + EPS_NORM)[:, None]
    own_hidden = (jax.nn.silu(factor * gate_part) * (factor * up_part)).astype(jnp.bfloat16)
    return collect(own_hidden, "kv", 0)


def advance(stream, inputs_back, weight_back, factor_branch):
    row_count = stream.shape[0] // lax.axis_size("tp")
    row_share = sent_and_summed(
        jnp.dot(inputs_back, weight_back, preferred_element_type=jnp.float32).astype(jnp.bfloat16),
        "tp",
        0,
    )
    own_rows = lax.dynamic_slice_in_dim(stream, lax.axis_index("tp") * row_count, row_count, 0)
    return (own_rows.astype(jnp.float32) + factor_branch * row_share).astype(jnp.bfloat16)


def rotate(values_in, cosine, sine_part):
    half_dim = values_in.shape[-1] // 2
    lower_half = values_in[..., :half_dim]
    upper_half = values_in[..., half_dim:]
    return jnp.concatenate(
        [
            lower_half * cosine - upper_half * sine_part,
            lower_half * sine_part + upper_half * cosine,
        ],
        axis=-1,
    )


def retention(
    stream, norm_gain, w_query, w_key, w_value, w_outgate, head_gain, state_old, positions
):
    squares, scaled = prepare(stream, norm_gain)
    query_part = jnp.dot(scaled, w_query, preferred_element_type=jnp.float32)
    key_part = jnp.dot(scaled, w_key, preferred_element_type=jnp.float32)
    value_part = jnp.dot(scaled, w_value, preferred_element_type=jnp.float32)
    gate_part = jnp.dot(scaled, w_outgate, preferred_element_type=jnp.float32)
    query_part, key_part, value_part, gate_part, squares = sent_together(
        (
            query_part.astype(jnp.bfloat16),
            key_part.astype(jnp.bfloat16),
            value_part.astype(jnp.bfloat16),
            gate_part.astype(jnp.bfloat16),
            squares.astype(jnp.bfloat16),
        ),
        "kv",
        0,
        1,
    )
    factor = lax.rsqrt(squares / D + EPS_NORM)[:, None]
    sequences = state_old.shape[0]
    head_count = state_old.shape[1]
    width_head = state_old.shape[2]
    shape_heads = (sequences, head_count, width_head)
    queries = (factor * query_part).reshape(shape_heads)
    key_vec = (factor * key_part).reshape(shape_heads)
    values_new = (factor * value_part).reshape(shape_heads)
    gate_pre = (factor * gate_part).reshape(shape_heads)
    half_dim = width_head // 2
    inverse = 10000.0 ** (-jnp.arange(half_dim, dtype=jnp.float32) / half_dim)
    angles = positions.astype(jnp.float32)[:, None] * inverse[None, :]
    cosine = jnp.cos(angles)[:, None, :]
    sine_part = jnp.sin(angles)[:, None, :]
    queries = rotate(queries, cosine, sine_part)
    key_vec = rotate(key_vec, cosine, sine_part) * width_head ** (-0.5)
    head_ids = (lax.axis_index("tp") * head_count + jnp.arange(head_count)).astype(jnp.float32)
    decays = jnp.exp(jnp.log1p(-(2.0 ** (-5.0 - head_ids))))
    carried = jnp.einsum("shd,shde->she", queries, state_old, precision=lax.Precision.HIGHEST)
    within = jnp.sum(queries * key_vec, axis=-1, keepdims=True)
    mixture = decays[None, :, None] * carried + within * values_new
    new_state = (
        decays[None, :, None, None] * state_old + key_vec[..., :, None] * values_new[..., None, :]
    )
    average = jnp.mean(mixture, axis=-1, keepdims=True)
    centered = mixture - average
    variance = jnp.mean(centered * centered, axis=-1, keepdims=True)
    normed = centered * lax.rsqrt(variance + EPS_GROUP) * head_gain.reshape(head_count, width_head)
    ret_out = (
        (jax.nn.silu(gate_pre) * normed)
        .astype(jnp.bfloat16)
        .reshape(sequences, head_count * width_head)
    )
    return (collect(ret_out, "kv", 0), new_state)


def per_device(
    stream_in,
    positions,
    ret_state,
    first_gain,
    first_gate,
    first_up,
    first_down,
    mix_gain,
    w_query,
    w_key,
    w_value,
    w_outgate,
    w_out,
    head_gain,
    second_gain,
    second_gate,
    second_up,
    second_down,
):
    stream = widen_rows(stream_in)
    hidden = feed_forward(stream, first_gain, first_gate, first_up)
    stream = advance(stream, hidden, first_down, 0.5)
    stream = widen_rows(stream)
    ret_out, new_state = retention(
        stream, mix_gain, w_query, w_key, w_value, w_outgate, head_gain, ret_state, positions
    )
    stream = advance(stream, ret_out, w_out, 1.0)
    stream = widen_rows(stream)
    hidden = feed_forward(stream, second_gain, second_gate, second_up)
    stream = advance(stream, hidden, second_down, 0.5)
    return (stream, new_state)


def solution(mesh):
    in_specs = (
        P(("grp", "tp"), "kv"),
        P(("grp", "kv")),
        P(("grp", "kv"), "tp", None, None),
        P("kv"),
        P("kv", "tp"),
        P("kv", "tp"),
        P("tp", "kv"),
        P("kv"),
        P("kv", "tp"),
        P("kv", "tp"),
        P("kv", "tp"),
        P("kv", "tp"),
        P("tp", "kv"),
        P("tp"),
        P("kv"),
        P("kv", "tp"),
        P("kv", "tp"),
        P("tp", "kv"),
    )
    out_specs = (P(("grp", "tp"), "kv"), P(("grp", "kv"), "tp", None, None))
    return jax.shard_map(
        per_device, mesh=mesh, in_specs=in_specs, out_specs=out_specs, check_vma=False
    )
```

profile of v0, /device:TPU:65, one launch (start us, length us, event | category | flops | bytes accessed | tf_op | source)
XLA Modules:
  0.0 336.0 jit_solution(10473639947356605988)
XLA Ops:
  0.6 56.3 %all-gather = bf16[16,12,256]{2,1,0:T(8,128)(2,1)S(1)} all-gather(bf16[1,12,256]{2,1,0:T(8,128)(2,1)} %bitcast.43), channel_id=1, replica_groups=mesh['grp'=2,'kv'=16,'tp'=16] {'tp'}, dimensions={0}, use_global_device_ids=true | all-gather | bytes 104448 | tf_op jit(solution)/shard_map/all_gather | solution.py:51
  57.1 0.2 convert_element_type.186
  57.4 1.0 convolution_convert_fusion.2
  58.4 0.3 convolution_convert_fusion.3
  58.8 0.5 concatenate.63
  59.3 42.3 %all_to_all.45 = bf16[16,12,1377]{2,1,0:T(8,128)(2,1)S(1)} all-to-all(bf16[16,12,1377]{2,1,0:T(8,128)(2,1)S(1)} %concatenate.63), channel_id=1, replica_groups=mesh['grp'=2,'kv'=16,'tp'=16] {'kv'}, dimensions={0} | all-to-all | bytes 1057536 | tf_op jit(solution)/shard_map/all_to_all | solution.py:19
  101.7 0.2 fusion.44
  102.1 26.0 %all_to_all.46 = bf16[16,12,688]{2,1,0:T(8,128)(2,1)S(1)} all-to-all(bf16[16,12,688]{2,1,0:T(8,128)(2,1)S(1)} %broadcast_in_dim.6), channel_id=1, replica_groups=mesh['grp'=2,'kv'=16,'tp'=16] {'kv'}, dimensions={0} | all-to-all | bytes 528384 | tf_op jit(solution)/shard_map/all_to_all | solution.py:36
  128.2 0.2 convolution_convert_fusion.6
  128.5 0.7 reshape.328
  129.1 11.7 %all-to-all-start.2 = ((bf16[16,12,256]{2,1,0:T(8,128)(2,1)}), bf16[16,12,256]{2,1,0:T(8,128)(2,1)S(1)}, u32[]{:S(2)}, u32[]{:S(2)}) async-start(bf16[16,12,256]{2,1,0:T(8,128)(2,1)} %reshape.328), calls=%async_computation.2 | async-start | bytes 262144 | tf_op jit(solution)/shard_map/all_to_all | solution.py:19
  140.8 8.9 %all-to-all-done.2 = bf16[16,12,256]{2,1,0:T(8,128)(2,1)S(1)} async-done(((bf16[16,12,256]{2,1,0:T(8,128)(2,1)}), bf16[16,12,256]{2,1,0:T(8,128)(2,1)S(1)}, u32[]{:S(2)}, u32[]{:S(2)}) %all-to-all-start.2) | async-done | bytes 98336 | tf_op jit(solution)/shard_map/all_to_all | solution.py:19
  149.8 14.9 %all-gather.1 = bf16[16,12,256]{2,1,0:T(8,128)(2,1)S(1)} all-gather(bf16[1,12,256]{2,1,0:T(8,128)(2,1)S(1)} %fusion.32), channel_id=1, replica_groups=mesh['grp'=2,'kv'=16,'tp'=16] {'tp'}, dimensions={0}, use_global_device_ids=true | all-gather | bytes 104448 | tf_op jit(solution)/shard_map/all_gather | solution.py:51
  164.8 0.2 convolution_convert_fusion.9
  165.0 0.2 convolution_convert_fusion.8
  165.2 0.2 convolution_convert_fusion.7
  165.4 0.2 convolution_convert_fusion.10
  165.6 0.2 convert_element_type.187
  165.9 0.6 constant_dynamic-update-slice_fusion.4
  166.5 0.6 constant_dynamic-update-slice_fusion.3
  167.2 0.6 constant_dynamic-update-slice_fusion.2
  167.8 0.6 constant_dynamic-update-slice_fusion.1
  168.4 0.6 constant_dynamic-update-slice_fusion
  169.1 5.7 %all-to-all-start.3 = ((bf16[16,12,513]{2,1,0:T(8,128)(2,1)}), bf16[16,12,513]{2,1,0:T(8,128)(2,1)S(1)}, u32[]{:S(2)}, u32[]{:S(2)}) async-start(bf16[16,12,513]{2,1,0:T(8,128)(2,1)} %constant_dynamic-update-slice_fusion), calls=%async_computation.3 | async-start | bytes 655360 | tf_op jit(solution)/shard_map/all_to_all | solution.py:19
  175.0 15.2 %all-to-all-done.3 = bf16[16,12,513]{2,1,0:T(8,128)(2,1)S(1)} async-done(((bf16[16,12,513]{2,1,0:T(8,128)(2,1)}), bf16[16,12,513]{2,1,0:T(8,128)(2,1)S(1)}, u32[]{:S(2)}, u32[]{:S(2)}) %all-to-all-start.3) | async-done | bytes 197024 | tf_op jit(solution)/shard_map/all_to_all | solution.py:19
  190.6 0.8 fusion
  191.4 0.3 fusion.48
  191.7 0.2 fusion.49
  191.9 0.2 multiply_reduce_fusion
  192.2 22.9 %all_to_all.47 = bf16[16,12,128]{2,1,0:T(8,128)(2,1)S(1)} all-to-all(bf16[16,12,128]{2,1,0:T(8,128)(2,1)S(1)} %broadcast_in_dim.7), channel_id=1, replica_groups=mesh['grp'=2,'kv'=16,'tp'=16] {'kv'}, dimensions={0} | all-to-all | bytes 98304 | tf_op jit(solution)/shard_map/all_to_all | solution.py:36
  215.4 15.6 %all_to_all.48 = bf16[16,12,256]{2,1,0:T(8,128)(2,1)S(1)} all-to-all(bf16[16,12,256]{2,1,0:T(8,128)(2,1)S(1)} %reshape.334), channel_id=1, replica_groups=mesh['grp'=2,'kv'=16,'tp'=16] {'tp'}, dimensions={0} | all-to-all | bytes 196608 | tf_op jit(solution)/shard_map/all_to_all | solution.py:19
  231.1 14.9 %all-gather.2 = bf16[16,12,256]{2,1,0:T(8,128)(2,1)S(1)} all-gather(bf16[1,12,256]{2,1,0:T(8,128)(2,1)S(1)} %fusion.33), channel_id=1, replica_groups=mesh['grp'=2,'kv'=16,'tp'=16] {'tp'}, dimensions={0}, use_global_device_ids=true | all-gather | bytes 104448 | tf_op jit(solution)/shard_map/all_gather | solution.py:51
  246.1 0.2 convert_element_type.188
  246.4 0.3 convolution_convert_fusion
  246.8 0.2 copy-done.5
  247.0 0.3 convolution_convert_fusion.1
  247.3 0.5 concatenate.73
  247.8 38.5 %all_to_all.49 = bf16[16,12,1377]{2,1,0:T(8,128)(2,1)S(1)} all-to-all(bf16[16,12,1377]{2,1,0:T(8,128)(2,1)S(1)} %concatenate.73), channel_id=1, replica_groups=mesh['grp'=2,'kv'=16,'tp'=16] {'kv'}, dimensions={0} | all-to-all | bytes 1057536 | tf_op jit(solution)/shard_map/all_to_all | solution.py:19
  286.5 0.2 fusion.36
  286.8 0.8 broadcast_in_dim.8
  287.6 8.4 %all-to-all-start.7 = ((bf16[16,12,688]{2,1,0:T(8,128)(2,1)}), bf16[16,12,688]{2,1,0:T(8,128)(2,1)S(1)}, u32[]{:S(2)}, u32[]{:S(2)}) async-start(bf16[16,12,688]{2,1,0:T(8,128)(2,1)} %broadcast_in_dim.8), calls=%async_computation.7 | async-start | bytes 786432 | tf_op jit(solution)/shard_map/all_to_all | solution.py:36
  296.1 17.5 %all-to-all-done.7 = bf16[16,12,688]{2,1,0:T(8,128)(2,1)S(1)} async-done(((bf16[16,12,688]{2,1,0:T(8,128)(2,1)}), bf16[16,12,688]{2,1,0:T(8,128)(2,1)S(1)}, u32[]{:S(2)}, u32[]{:S(2)}) %all-to-all-start.7) | async-done | bytes 264224 | tf_op jit(solution)/shard_map/all_to_all | solution.py:36
  313.7 0.2 convolution_convert_fusion.4
  314.0 0.7 reshape.336
  314.7 11.8 %all-to-all-start.8 = ((bf16[16,12,256]{2,1,0:T(8,128)(2,1)}), bf16[16,12,256]{2,1,0:T(8,128)(2,1)S(1)}, u32[]{:S(2)}, u32[]{:S(2)}) async-start(bf16[16,12,256]{2,1,0:T(8,128)(2,1)} %reshape.336), calls=%async_computation.8 | async-start | bytes 262144 | tf_op jit(solution)/shard_map/all_to_all | solution.py:19
  326.4 1.2 multiply_add_fusion
  327.6 7.7 %all-to-all-done.8 = bf16[16,12,256]{2,1,0:T(8,128)(2,1)S(1)} async-done(((bf16[16,12,256]{2,1,0:T(8,128)(2,1)}), bf16[16,12,256]{2,1,0:T(8,128)(2,1)S(1)}, u32[]{:S(2)}, u32[]{:S(2)}) %all-to-all-start.8) | async-done | bytes 98336 | tf_op jit(solution)/shard_map/all_to_all | solution.py:19
  335.4 0.6 add_convert_fusion
  (77 shorter events, 2.5 us)
Async XLA Ops:
  0.6 56.7 %copy-start = (bf16[256,688]{0,1:T(8,128)(2,1)S(1)}, bf16[256,688]{0,1:T(8,128)(2,1)}, u32[]{:S(2)}) copy-start(bf16[256,688]{0,1:T(8,128)(2,1)} %param.23) | copy-start | bytes 1056772
  57.0 1.4 copy-start.2
  57.0 1.4 copy-start.13
  102.1 26.1 %copy-start.3 = (bf16[688,256]{1,0:T(8,128)(2,1)S(1)}, bf16[688,256]{1,0:T(8,128)(2,1)}, u32[]{:S(2)}) copy-start(bf16[688,256]{1,0:T(8,128)(2,1)} %param.24) | copy-start | bytes 1056772
  128.2 36.6 %copy-start.7 = (bf16[256,128]{1,0:T(8,128)(2,1)S(1)}, bf16[256,128]{1,0:T(8,128)(2,1)}, u32[]{:S(2)}) copy-start(bf16[256,128]{1,0:T(8,128)(2,1)} %param.27) | copy-start | bytes 196612
  128.2 36.6 %copy-start.12 = (f32[256]{0:T(256)S(1)}, f32[256]{0:T(256)}, u32[]{:S(2)}) copy-start(f32[256]{0:T(256)} %param.25) | copy-start | bytes 3076
  128.4 36.6 %copy-start.8 = (bf16[256,128]{1,0:T(8,128)(2,1)S(1)}, bf16[256,128]{1,0:T(8,128)(2,1)}, u32[]{:S(2)}) copy-start(bf16[256,128]{1,0:T(8,128)(2,1)} %param.28) | copy-start | bytes 196612
  129.1 36.1 %copy-start.9 = (bf16[256,128]{1,0:T(8,128)(2,1)S(1)}, bf16[256,128]{1,0:T(8,128)(2,1)}, u32[]{:S(2)}) copy-start(bf16[256,128]{1,0:T(8,128)(2,1)} %param.29) | copy-start | bytes 196612
  129.1 20.6 %all-to-all-start.2 = ((bf16[16,12,256]{2,1,0:T(8,128)(2,1)}), bf16[16,12,256]{2,1,0:T(8,128)(2,1)S(1)}, u32[]{:S(2)}, u32[]{:S(2)}) async-start(bf16[16,12,256]{2,1,0:T(8,128)(2,1)} %reshape.328), calls=%async_computation.2 | async-start | bytes 262144 | tf_op jit(solution)/shard_map/all_to_all | solution.py:19
  140.8 24.6 %copy-start.10 = (bf16[256,128]{1,0:T(8,128)(2,1)S(1)}, bf16[256,128]{1,0:T(8,128)(2,1)}, u32[]{:S(2)}) copy-start(bf16[256,128]{1,0:T(8,128)(2,1)} %param.26) | copy-start | bytes 196612
  165.6 9.3 %copy-start.16 = (s32[12]{0:T(128)S(1)}, s32[12]{0:T(128)}, u32[]{:S(2)}) copy-start(s32[12]{0:T(128)} %param.19) | copy-start | bytes 148
  167.1 23.5 %copy-start.1 = (f32[12,1,128,128]{3,2,1,0:T(8,128)S(1)}, f32[12,1,128,128]{3,2,1,0:T(8,128)}, u32[]{:S(2)}) copy-start(f32[12,1,128,128]{3,2,1,0:T(8,128)} %param.20) | copy-start | bytes 2359300
  169.1 21.1 %all-to-all-start.3 = ((bf16[16,12,513]{2,1,0:T(8,128)(2,1)}), bf16[16,12,513]{2,1,0:T(8,128)(2,1)S(1)}, u32[]{:S(2)}, u32[]{:S(2)}) async-start(bf16[16,12,513]{2,1,0:T(8,128)(2,1)} %constant_dynamic-update-slice_fusion), calls=%async_computation.3 | async-start | bytes 655360 | tf_op jit(solution)/shard_map/all_to_all | solution.py:19
  174.8 17.3 %copy-start.15 = (f32[128]{0:T(128)S(1)}, f32[128]{0:T(128)}, u32[]{:S(2)}) copy-start(f32[128]{0:T(128)} %param.31) | copy-start | bytes 1540
  190.2 25.0 %copy-start.11 = (bf16[128,256]{1,0:T(8,128)(2,1)S(1)}, bf16[128,256]{1,0:T(8,128)(2,1)}, u32[]{:S(2)}) copy-start(bf16[128,256]{1,0:T(8,128)(2,1)} %param.30) | copy-start | bytes 196612
  215.1 31.2 %copy-start.4 = (bf16[256,688]{0,1:T(8,128)(2,1)S(1)}, bf16[256,688]{0,1:T(8,128)(2,1)}, u32[]{:S(2)}) copy-start(bf16[256,688]{0,1:T(8,128)(2,1)} %param.34) | copy-start | bytes 1056772
  215.1 31.3 %copy-start.14 = (f32[256]{0:T(256)S(1)}, f32[256]{0:T(256)}, u32[]{:S(2)}) copy-start(f32[256]{0:T(256)} %param.32) | copy-start | bytes 3076
  246.0 1.0 copy-start.5
  287.6 26.2 %copy-start.6 = (bf16[688,256]{1,0:T(8,128)(2,1)S(1)}, bf16[688,256]{1,0:T(8,128)(2,1)}, u32[]{:S(2)}) copy-start(bf16[688,256]{1,0:T(8,128)(2,1)} %param.35) | copy-start | bytes 1056772
  287.6 26.0 %all-to-all-start.7 = ((bf16[16,12,688]{2,1,0:T(8,128)(2,1)}), bf16[16,12,688]{2,1,0:T(8,128)(2,1)S(1)}, u32[]{:S(2)}, u32[]{:S(2)}) async-start(bf16[16,12,688]{2,1,0:T(8,128)(2,1)} %broadcast_in_dim.8), calls=%async_computation.7 | async-start | bytes 786432 | tf_op jit(solution)/shard_map/all_to_all | solution.py:36
  314.7 20.7 %all-to-all-start.8 = ((bf16[16,12,256]{2,1,0:T(8,128)(2,1)}), bf16[16,12,256]{2,1,0:T(8,128)(2,1)S(1)}, u32[]{:S(2)}, u32[]{:S(2)}) async-start(bf16[16,12,256]{2,1,0:T(8,128)(2,1)} %reshape.336), calls=%async_computation.8 | async-start | bytes 262144 | tf_op jit(solution)/shard_map/all_to_all | solution.py:19
where the time goes:
time: 337 us; the launch traced here: 336 us
  blocking collectives  232 us (69%)
  waiting for transfers between devices  49.3 us (15%)
  starting transfers between devices  37.6 us (11%)
  local copies, waits for them, and re-layouts  8.12 us (2%)
  other arithmetic  4.29 us (1%)
  matrix products  3.82 us (1%)
    all_to_all x3, blocking collectives, sent_and_summed(): lax.all_to_all(parts, axis, split_axis=0, concat_axis=0, tiled=True)  96.5 us
    all_gather x3, blocking collectives, widen_rows(): return lax.all_gather(stream_rows, 'tp', axis=0, tiled=True)  86.1 us
    all_to_all x2, blocking collectives, from_everyone(): lax.all_to_all(jnp.broadcast_to(x[None], (length, *x.shape)), axis, 0, 0,...  48.9 us
    all_to_all x3, waiting for transfers between devices, sent_and_summed(): lax.all_to_all(parts, axis, split_axis=0, concat_axis=0, tiled=True)  31.8 us
    all_to_all x3, starting transfers between devices, sent_and_summed(): lax.all_to_all(parts, axis, split_axis=0, concat_axis=0, tiled=True)  29.2 us
    all_to_all x1, waiting for transfers between devices, from_everyone(): lax.all_to_all(jnp.broadcast_to(x[None], (length, *x.shape)), axis, 0, 0,...  17.5 us
    all_to_all x1, starting transfers between devices, from_everyone(): lax.all_to_all(jnp.broadcast_to(x[None], (length, *x.shape)), axis, 0, 0,...  8.45 us
  transfers between devices with their start and end apart: 4, of which 4 were waited for; matrix products, arithmetic and copies ran while one was open for 0% of the time, Pallas kernels for 0%

commit v1 on v0

--- a/solution.py
+++ b/solution.py
@@ -48,7 +48,9 @@
 
 
 def widen_rows(stream_rows):
-    return lax.all_gather(stream_rows, "tp", axis=0, tiled=True)
+    return jnp.concatenate(
+        lax.all_to_all(jnp.stack([stream_rows] * lax.axis_size("tp")), "tp", 0, 0), axis=0
+    )
 
 
 def prepare(stream, norm_gain):

time: 337 us -> 325 us (0.964)
  blocking collectives: 232 us -> 220 us
    all_gather x3 -> x0, blocking collectives: 86.1 us -> none  [widen_rows(): return lax.all_gather(stream_rows, 'tp', axis=0, tiled=True)]
    all_to_all x0 -> x3, blocking collectives: none -> 75.7 us  [widen_rows(): lax.all_to_all(jnp.stack([stream_rows] * lax.axis_size('tp')), 'tp', 0, 0)]
where the time goes in v1:
time: 325 us; the launch traced here: 324 us
  blocking collectives  220 us (68%)
  waiting for transfers between devices  51.5 us (16%)
  starting transfers between devices  34.5 us (11%)
  local copies, waits for them, and re-layouts  9.73 us (3%)
  other arithmetic  4.28 us (1%)
    all_to_all x3, blocking collectives, sent_and_summed(): lax.all_to_all(parts, axis, split_axis=0, concat_axis=0, tiled=True)  96.9 us
    all_to_all x3, blocking collectives, widen_rows(): lax.all_to_all(jnp.stack([stream_rows] * lax.axis_size('tp')), 'tp', 0, 0)  75.7 us
    all_to_all x2, blocking collectives, from_everyone(): lax.all_to_all(jnp.broadcast_to(x[None], (length, *x.shape)), axis, 0, 0,...  47 us
    all_to_all x3, waiting for transfers between devices, sent_and_summed(): lax.all_to_all(parts, axis, split_axis=0, concat_axis=0, tiled=True)  34.1 us
    all_to_all x3, starting transfers between devices, sent_and_summed(): lax.all_to_all(parts, axis, split_axis=0, concat_axis=0, tiled=True)  27 us
    all_to_all x1, waiting for transfers between devices, from_everyone(): lax.all_to_all(jnp.broadcast_to(x[None], (length, *x.shape)), axis, 0, 0,...  17.4 us
    all_to_all x1, starting transfers between devices, from_everyone(): lax.all_to_all(jnp.broadcast_to(x[None], (length, *x.shape)), axis, 0, 0,...  7.48 us
  transfers between devices with their start and end apart: 4, of which 4 were waited for; matrix products, arithmetic and copies ran while one was open for 0% of the time, Pallas kernels for 0%

profile of v1, /device:TPU:65, one launch (start us, length us, event | category | flops | bytes accessed | tf_op | source)
XLA Modules:
  0.0 324.1 jit_solution(5338796926630746258)
XLA Ops:
  0.7 0.8 stack.6
  1.4 53.1 %all_to_all.60 = bf16[16,12,256]{2,1,0:T(8,128)(2,1)S(1)} all-to-all(bf16[16,12,256]{2,1,0:T(8,128)(2,1)S(1)} %stack.6), channel_id=1, replica_groups=mesh['grp'=2,'kv'=16,'tp'=16] {'tp'}, dimensions={0} | all-to-all | bytes 196608 | tf_op jit(solution)/shard_map/all_to_all | solution.py:52
  54.6 0.2 copy.40
  54.9 0.3 convolution_convert_fusion.2
  55.3 0.6 copy-done.2
  55.8 0.3 convolution_convert_fusion.3
  56.2 0.5 concatenate.63
  56.7 43.3 %all_to_all.61 = bf16[16,12,1377]{2,1,0:T(8,128)(2,1)S(1)} all-to-all(bf16[16,12,1377]{2,1,0:T(8,128)(2,1)S(1)} %concatenate.63), channel_id=1, replica_groups=mesh['grp'=2,'kv'=16,'tp'=16] {'kv'}, dimensions={0} | all-to-all | bytes 1057536 | tf_op jit(solution)/shard_map/all_to_all | solution.py:19
  100.1 0.2 fusion.28
  100.4 25.6 %all_to_all.62 = bf16[16,12,688]{2,1,0:T(8,128)(2,1)S(1)} all-to-all(bf16[16,12,688]{2,1,0:T(8,128)(2,1)S(1)} %broadcast_in_dim.6), channel_id=1, replica_groups=mesh['grp'=2,'kv'=16,'tp'=16] {'kv'}, dimensions={0} | all-to-all | bytes 528384 | tf_op jit(solution)/shard_map/all_to_all | solution.py:36
  126.2 0.2 convolution_convert_fusion.6
  126.5 0.7 reshape.341
  127.2 10.7 %all-to-all-start.3 = ((bf16[16,12,256]{2,1,0:T(8,128)(2,1)}), bf16[16,12,256]{2,1,0:T(8,128)(2,1)S(1)}, u32[]{:S(2)}, u32[]{:S(2)}) async-start(bf16[16,12,256]{2,1,0:T(8,128)(2,1)} %reshape.341), calls=%async_computation.3 | async-start | bytes 262144 | tf_op jit(solution)/shard_map/all_to_all | solution.py:19
  137.9 9.2 %all-to-all-done.3 = bf16[16,12,256]{2,1,0:T(8,128)(2,1)S(1)} async-done(((bf16[16,12,256]{2,1,0:T(8,128)(2,1)}), bf16[16,12,256]{2,1,0:T(8,128)(2,1)S(1)}, u32[]{:S(2)}, u32[]{:S(2)}) %all-to-all-start.3) | async-done | bytes 98336 | tf_op jit(solution)/shard_map/all_to_all | solution.py:19
  147.2 11.3 %all_to_all.63 = bf16[16,12,256]{2,1,0:T(8,128)(2,1)S(1)} all-to-all(bf16[16,12,256]{2,1,0:T(8,128)(2,1)S(1)} %stack.7), channel_id=1, replica_groups=mesh['grp'=2,'kv'=16,'tp'=16] {'tp'}, dimensions={0} | all-to-all | bytes 196608 | tf_op jit(solution)/shard_map/all_to_all | solution.py:52
  158.8 0.2 convolution_convert_fusion.8
  159.1 0.2 convolution_convert_fusion.10
  159.5 0.2 copy.41
  159.7 0.6 constant_dynamic-update-slice_fusion.4
  160.3 0.6 constant_dynamic-update-slice_fusion.3
  161.0 0.6 constant_dynamic-update-slice_fusion.2
  161.6 0.6 constant_dynamic-update-slice_fusion.1
  162.2 0.6 constant_dynamic-update-slice_fusion
  162.9 5.7 %all-to-all-start.5 = ((bf16[16,12,513]{2,1,0:T(8,128)(2,1)}), bf16[16,12,513]{2,1,0:T(8,128)(2,1)S(1)}, u32[]{:S(2)}, u32[]{:S(2)}) async-start(bf16[16,12,513]{2,1,0:T(8,128)(2,1)} %constant_dynamic-update-slice_fusion), calls=%async_computation.5 | async-start | bytes 655360 | tf_op jit(solution)/shard_map/all_to_all | solution.py:19
  168.8 16.8 %all-to-all-done.5 = bf16[16,12,513]{2,1,0:T(8,128)(2,1)S(1)} async-done(((bf16[16,12,513]{2,1,0:T(8,128)(2,1)}), bf16[16,12,513]{2,1,0:T(8,128)(2,1)S(1)}, u32[]{:S(2)}, u32[]{:S(2)}) %all-to-all-start.5) | async-done | bytes 197024 | tf_op jit(solution)/shard_map/all_to_all | solution.py:19
  186.0 0.8 fusion
  186.8 0.3 fusion.32
  187.1 0.2 fusion.33
  187.3 0.2 multiply_reduce_fusion.3
  187.6 21.4 %all_to_all.64 = bf16[16,12,128]{2,1,0:T(8,128)(2,1)S(1)} all-to-all(bf16[16,12,128]{2,1,0:T(8,128)(2,1)S(1)} %broadcast_in_dim.7), channel_id=1, replica_groups=mesh['grp'=2,'kv'=16,'tp'=16] {'kv'}, dimensions={0} | all-to-all | bytes 98304 | tf_op jit(solution)/shard_map/all_to_all | solution.py:36
  209.2 14.1 %all_to_all.65 = bf16[16,12,256]{2,1,0:T(8,128)(2,1)S(1)} all-to-all(bf16[16,12,256]{2,1,0:T(8,128)(2,1)S(1)} %reshape.348), channel_id=1, replica_groups=mesh['grp'=2,'kv'=16,'tp'=16] {'tp'}, dimensions={0} | all-to-all | bytes 196608 | tf_op jit(solution)/shard_map/all_to_all | solution.py:19
  223.4 11.3 %all_to_all.66 = bf16[16,12,256]{2,1,0:T(8,128)(2,1)S(1)} all-to-all(bf16[16,12,256]{2,1,0:T(8,128)(2,1)S(1)} %stack.8), channel_id=1, replica_groups=mesh['grp'=2,'kv'=16,'tp'=16] {'tp'}, dimensions={0} | all-to-all | bytes 196608 | tf_op jit(solution)/shard_map/all_to_all | solution.py:52
  234.8 0.2 copy.46
  235.1 0.3 convolution_convert_fusion
  235.5 0.6 copy-done.5
  236.0 0.3 convolution_convert_fusion.1
  236.4 0.5 concatenate.73
  236.9 39.5 %all_to_all.67 = bf16[16,12,1377]{2,1,0:T(8,128)(2,1)S(1)} all-to-all(bf16[16,12,1377]{2,1,0:T(8,128)(2,1)S(1)} %concatenate.73), channel_id=1, replica_groups=mesh['grp'=2,'kv'=16,'tp'=16] {'kv'}, dimensions={0} | all-to-all | bytes 1057536 | tf_op jit(solution)/shard_map/all_to_all | solution.py:19
  276.6 0.2 fusion.20
  276.9 0.8 broadcast_in_dim.8
  277.6 7.5 %all-to-all-start.10 = ((bf16[16,12,688]{2,1,0:T(8,128)(2,1)}), bf16[16,12,688]{2,1,0:T(8,128)(2,1)S(1)}, u32[]{:S(2)}, u32[]{:S(2)}) async-start(bf16[16,12,688]{2,1,0:T(8,128)(2,1)} %broadcast_in_dim.8), calls=%async_computation.10 | async-start | bytes 786432 | tf_op jit(solution)/shard_map/all_to_all | solution.py:36
  285.2 17.4 %all-to-all-done.10 = bf16[16,12,688]{2,1,0:T(8,128)(2,1)S(1)} async-done(((bf16[16,12,688]{2,1,0:T(8,128)(2,1)}), bf16[16,12,688]{2,1,0:T(8,128)(2,1)S(1)}, u32[]{:S(2)}, u32[]{:S(2)}) %all-to-all-start.10) | async-done | bytes 264224 | tf_op jit(solution)/shard_map/all_to_all | solution.py:36
  302.7 0.2 convolution_convert_fusion.4
  303.0 0.7 reshape.351
  303.6 10.6 %all-to-all-start.11 = ((bf16[16,12,256]{2,1,0:T(8,128)(2,1)}), bf16[16,12,256]{2,1,0:T(8,128)(2,1)S(1)}, u32[]{:S(2)}, u32[]{:S(2)}) async-start(bf16[16,12,256]{2,1,0:T(8,128)(2,1)} %reshape.351), calls=%async_computation.11 | async-start | bytes 262144 | tf_op jit(solution)/shard_map/all_to_all | solution.py:19
  314.2 1.1 multiply_add_fusion
  315.4 8.1 %all-to-all-done.11 = bf16[16,12,256]{2,1,0:T(8,128)(2,1)S(1)} async-done(((bf16[16,12,256]{2,1,0:T(8,128)(2,1)}), bf16[16,12,256]{2,1,0:T(8,128)(2,1)S(1)}, u32[]{:S(2)}, u32[]{:S(2)}) %all-to-all-start.11) | async-done | bytes 98336 | tf_op jit(solution)/shard_map/all_to_all | solution.py:19
  323.5 0.6 add_convert_fusion
  (80 shorter events, 2.9 us)
Async XLA Ops:
  0.6 54.3 %copy-start = (bf16[256,688]{0,1:T(8,128)(2,1)S(1)}, bf16[256,688]{0,1:T(8,128)(2,1)}, u32[]{:S(2)}) copy-start(bf16[256,688]{0,1:T(8,128)(2,1)} %param.23) | copy-start | bytes 1056772
  0.6 54.3 %copy-start.13 = (f32[256]{0:T(256)S(1)}, f32[256]{0:T(256)}, u32[]{:S(2)}) copy-start(f32[256]{0:T(256)} %param.21) | copy-start | bytes 3076
  54.9 1.0 copy-start.2
  100.4 25.8 %copy-start.3 = (bf16[688,256]{1,0:T(8,128)(2,1)S(1)}, bf16[688,256]{1,0:T(8,128)(2,1)}, u32[]{:S(2)}) copy-start(bf16[688,256]{1,0:T(8,128)(2,1)} %param.24) | copy-start | bytes 1056772
  126.4 32.1 %copy-start.7 = (bf16[256,128]{1,0:T(8,128)(2,1)S(1)}, bf16[256,128]{1,0:T(8,128)(2,1)}, u32[]{:S(2)}) copy-start(bf16[256,128]{1,0:T(8,128)(2,1)} %param.27) | copy-start | bytes 196612
  126.4 32.1 %copy-start.12 = (f32[256]{0:T(256)S(1)}, f32[256]{0:T(256)}, u32[]{:S(2)}) copy-start(f32[256]{0:T(256)} %param.25) | copy-start | bytes 3076
  126.5 32.3 %copy-start.8 = (bf16[256,128]{1,0:T(8,128)(2,1)S(1)}, bf16[256,128]{1,0:T(8,128)(2,1)}, u32[]{:S(2)}) copy-start(bf16[256,128]{1,0:T(8,128)(2,1)} %param.28) | copy-start | bytes 196612
  127.2 19.9 %all-to-all-start.3 = ((bf16[16,12,256]{2,1,0:T(8,128)(2,1)}), bf16[16,12,256]{2,1,0:T(8,128)(2,1)S(1)}, u32[]{:S(2)}, u32[]{:S(2)}) async-start(bf16[16,12,256]{2,1,0:T(8,128)(2,1)} %reshape.341), calls=%async_computation.3 | async-start | bytes 262144 | tf_op jit(solution)/shard_map/all_to_all | solution.py:19
  137.8 21.1 %copy-start.9 = (bf16[256,128]{1,0:T(8,128)(2,1)S(1)}, bf16[256,128]{1,0:T(8,128)(2,1)}, u32[]{:S(2)}) copy-start(bf16[256,128]{1,0:T(8,128)(2,1)} %param.29) | copy-start | bytes 196612
  147.2 12.0 %copy-start.10 = (bf16[256,128]{1,0:T(8,128)(2,1)S(1)}, bf16[256,128]{1,0:T(8,128)(2,1)}, u32[]{:S(2)}) copy-start(bf16[256,128]{1,0:T(8,128)(2,1)} %param.26) | copy-start | bytes 196612
  159.3 9.4 %copy-start.16 = (s32[12]{0:T(128)S(1)}, s32[12]{0:T(128)}, u32[]{:S(2)}) copy-start(s32[12]{0:T(128)} %param.19) | copy-start | bytes 148
  161.0 25.0 %copy-start.1 = (f32[12,1,128,128]{3,2,1,0:T(8,128)S(1)}, f32[12,1,128,128]{3,2,1,0:T(8,128)}, u32[]{:S(2)}) copy-start(f32[12,1,128,128]{3,2,1,0:T(8,128)} %param.20) | copy-start | bytes 2359300
  162.9 22.7 %all-to-all-start.5 = ((bf16[16,12,513]{2,1,0:T(8,128)(2,1)}), bf16[16,12,513]{2,1,0:T(8,128)(2,1)S(1)}, u32[]{:S(2)}, u32[]{:S(2)}) async-start(bf16[16,12,513]{2,1,0:T(8,128)(2,1)} %constant_dynamic-update-slice_fusion), calls=%async_computation.5 | async-start | bytes 655360 | tf_op jit(solution)/shard_map/all_to_all | solution.py:19
  168.6 18.9 %copy-start.15 = (f32[128]{0:T(128)S(1)}, f32[128]{0:T(128)}, u32[]{:S(2)}) copy-start(f32[128]{0:T(128)} %param.31) | copy-start | bytes 1540
  185.6 23.4 %copy-start.11 = (bf16[128,256]{1,0:T(8,128)(2,1)S(1)}, bf16[128,256]{1,0:T(8,128)(2,1)}, u32[]{:S(2)}) copy-start(bf16[128,256]{1,0:T(8,128)(2,1)} %param.30) | copy-start | bytes 196612
  209.2 25.9 %copy-start.4 = (bf16[256,688]{0,1:T(8,128)(2,1)S(1)}, bf16[256,688]{0,1:T(8,128)(2,1)}, u32[]{:S(2)}) copy-start(bf16[256,688]{0,1:T(8,128)(2,1)} %param.34) | copy-start | bytes 1056772
  209.2 25.9 %copy-start.14 = (f32[256]{0:T(256)S(1)}, f32[256]{0:T(256)}, u32[]{:S(2)}) copy-start(f32[256]{0:T(256)} %param.32) | copy-start | bytes 3076
  235.0 1.0 copy-start.5
  277.6 25.1 %copy-start.6 = (bf16[688,256]{1,0:T(8,128)(2,1)S(1)}, bf16[688,256]{1,0:T(8,128)(2,1)}, u32[]{:S(2)}) copy-start(bf16[688,256]{1,0:T(8,128)(2,1)} %param.35) | copy-start | bytes 1056772
  277.6 25.0 %all-to-all-start.10 = ((bf16[16,12,688]{2,1,0:T(8,128)(2,1)}), bf16[16,12,688]{2,1,0:T(8,128)(2,1)S(1)}, u32[]{:S(2)}, u32[]{:S(2)}) async-start(bf16[16,12,688]{2,1,0:T(8,128)(2,1)} %broadcast_in_dim.8), calls=%async_computation.10 | async-start | bytes 786432 | tf_op jit(solution)/shard_map/all_to_all | solution.py:36
  303.6 19.8 %all-to-all-start.11 = ((bf16[16,12,256]{2,1,0:T(8,128)(2,1)}), bf16[16,12,256]{2,1,0:T(8,128)(2,1)S(1)}, u32[]{:S(2)}, u32[]{:S(2)}) async-start(bf16[16,12,256]{2,1,0:T(8,128)(2,1)} %reshape.351), calls=%async_computation.11 | async-start | bytes 262144 | tf_op jit(solution)/shard_map/all_to_all | solution.py:19
